TPU v7x, 32 devices: a whole 2x2x4 slice. The times are simulated.
32 devices in a mesh: grp: 2 (over y), sp: 4 (over z), tp: 4 (over x, core).
Axes of the slice: x: 2, y: 2, z: 4, core: 2. Of those that a mesh axis runs over, the one named last changes fastest.
Arguments:
- target: bfloat16 [1024, 2048], P(('grp', 'sp', 'tp')), parts along dimension 0, may hold values from -5 to 5
- source: bfloat16 [8192, 2048], P(('grp', 'sp', 'tp')), parts along dimension 0, may hold values from -5 to 5
- source_gain: float32 [2048], replicated, may hold values from 0.1 to 1.9
- pre_first: float32 [2048], replicated, may hold values from 0.1 to 1.9
- query_first: bfloat16 [2048, 2048], P(None, 'tp')
- keyval_first: bfloat16 [2048, 1024], P(None, 'tp')
- out_first: bfloat16 [2048, 2048], P('tp'), may hold values from -0.125 to 0.125
- post_first: float32 [2048], replicated, may hold values from 0.1 to 1.9
- ffn_pre: float32 [2048], replicated, may hold values from 0.1 to 1.9
- w_gate: bfloat16 [2048, 2816], P(None, 'tp'), may hold values from -0.125 to 0.125
- w_value: bfloat16 [2048, 2816], P(None, 'tp'), may hold values from -0.125 to 0.125
- conv_gate: float32 [3, 2816], P(None, 'tp'), may hold values from -3.5 to 3.5
- conv_value: float32 [3, 2816], P(None, 'tp'), may hold values from -3.5 to 3.5
- w_down: bfloat16 [2816, 2048], P('tp'), may hold values from -0.109375 to 0.109375
- ffn_post: float32 [2048], replicated, may hold values from 0.1 to 1.9
- pre_second: float32 [2048], replicated, may hold values from 0.1 to 1.9
- query_second: bfloat16 [2048, 2048], P(None, 'tp')
- keyval_second: bfloat16 [2048, 1024], P(None, 'tp')
- out_second: bfloat16 [2048, 2048], P('tp'), may hold values from -0.125 to 0.125
- post_second: float32 [2048], replicated, may hold values from 0.1 to 1.9
Outputs:
- decoded: float32 [1024, 2048], P(('grp', 'sp', 'tp')), parts along dimension 0
There are 2 independent parts, one for each index of `grp`. A program takes and returns all parts, laid end to end along the dimension named above; an argument that names none is the same for every part. Nothing has to cross between parts.
All inputs are finite; a program needn't handle non-finite values.
Results may differ from a plain program's by a relative error of at most 0.04.
Values may be sent and summed in bfloat16 or wider, within the bound.
A program may use at most 128 MiB of HBM per device.

v0:
```python
import jax
import jax.numpy as jnp
from jax import lax
from jax.sharding import PartitionSpec as P

HEAD = 128


def swapped(block, axis, distance):
    count = lax.axis_size(axis)
    route = []
    for low in range(count):
        high = low | 1 << distance
        if high != low and high < count:
            route += [(low, high), (high, low)]
    return lax.ppermute(block, axis, route)


def shifted(value, axis, steps):
    count = lax.axis_size(axis)
    leading, last = (max(0, -steps), min(count, count - steps))
    return lax.ppermute(value, axis, [(source, source + steps) for source in range(leading, last)])


def normed(values, gain):
    widened = values.astype(jnp.float32)
    return widened * lax.rsqrt(jnp.mean(widened * widened, axis=-1, keepdims=True) + 1e-06) * gain


def project_rows(rows_here, weights):
    shard_rows = lax.all_gather(rows_here, "tp", axis=0, tiled=True)
    products = [
        jnp.dot(shard_rows, weight, preferred_element_type=jnp.float32).astype(jnp.bfloat16)
        for weight in weights
    ]
    return jnp.concatenate(products, axis=1)


def summed_rows(parts, weight):
    return lax.psum_scatter(
        jnp.dot(parts, weight, preferred_element_type=jnp.float32).astype(jnp.bfloat16),
        "tp",
        scatter_dimension=0,
        tiled=True,
    ).astype(jnp.float32)


def key_columns(source_rows, keyval_first, keyval_second):
    both_layers = jnp.concatenate([keyval_first, keyval_second], axis=1)
    columns = jnp.einsum(
        "rd,dc->cr",
        lax.all_gather(source_rows, "tp", axis=0, tiled=True),
        both_layers,
        preferred_element_type=jnp.float32,
    ).astype(jnp.bfloat16)
    column_count = keyval_first.shape[1]
    stacked = columns.reshape(2, column_count, columns.shape[1])
    own_index = lax.axis_index("tp")
    doublings = (2 * HEAD // column_count).bit_length() - 1
    for bit_number in range(doublings):
        lower_half = own_index // 2**bit_number % 2 == 0
        outgoing = stacked
        retained = stacked
        partner = swapped(outgoing, "tp", bit_number)
        stacked = jnp.where(
            lower_half,
            jnp.concatenate([retained, partner], axis=1),
            jnp.concatenate([partner, retained], axis=1),
        )
    return (stacked[:, :HEAD], stacked[:, HEAD:])


def absorber(query_heads, running, shard_pair):
    scale_factor = HEAD ** (-0.5)
    best_score, weight_sum, weighted = running
    key_block, value_block = shard_pair
    scores = (
        jnp.einsum("thd,ds->ths", query_heads, key_block, preferred_element_type=jnp.float32)
        * scale_factor
    )
    newest = jnp.max(scores, axis=2)
    rescale = jnp.exp(best_score - newest)
    weights = jnp.exp(scores - newest[:, :, None])
    weight_sum = weight_sum * rescale + jnp.sum(weights, axis=2)
    weighted = weighted * rescale[:, :, None] + jnp.einsum(
        "ths,ds->thd", weights.astype(jnp.bfloat16), value_block, preferred_element_type=jnp.float32
    )
    return (newest, weight_sum, weighted)


def empty_running(row_count, head_count):
    return (
        jnp.full((row_count, head_count), -jnp.inf, jnp.float32),
        jnp.zeros((row_count, head_count), jnp.float32),
        jnp.zeros((row_count, head_count, HEAD), jnp.float32),
    )


def attend_keys(queries, keys_t, values_t):
    row_count = queries.shape[0]
    head_count = queries.shape[1] // HEAD
    query_heads = queries.reshape(row_count, head_count, HEAD)
    best_score, weight_sum, weighted = absorber(
        query_heads,
        empty_running(row_count, head_count),
        (
            lax.all_gather(keys_t, "sp", axis=1, tiled=True),
            lax.all_gather(values_t, "sp", axis=1, tiled=True),
        ),
    )
    return (
        (weighted / weight_sum[:, :, None])
        .reshape(row_count, head_count * HEAD)
        .astype(jnp.bfloat16)
    )


def causal_mix(rim_rows, up_rows, conv_taps):
    padded = jnp.concatenate([rim_rows, up_rows], axis=0).astype(jnp.float32)
    length = up_rows.shape[0]
    return (
        conv_taps[0] * padded[:length]
        + conv_taps[1] * padded[1 : length + 1]
        + conv_taps[2] * padded[2:]
    )


def per_device(
    target,
    source,
    source_gain,
    pre_first,
    query_first,
    keyval_first,
    out_first,
    post_first,
    ffn_pre,
    w_gate,
    w_value,
    conv_gate,
    conv_value,
    w_down,
    ffn_post,
    pre_second,
    query_second,
    keyval_second,
    out_second,
    post_second,
):
    source_rows = normed(source, source_gain).astype(jnp.bfloat16)
    keys_t, values_t = key_columns(source_rows, keyval_first, keyval_second)

    def attention_layer(stream, pre_gain, w_query, layer_index, w_out, post_gain):
        queries = project_rows(normed(stream, pre_gain).astype(jnp.bfloat16), (w_query,))
        heads = attend_keys(queries, keys_t[layer_index], values_t[layer_index])
        mixed = summed_rows(heads, w_out)
        return stream.astype(jnp.float32) + normed(mixed, post_gain)

    after_first = attention_layer(target, pre_first, query_first, 0, out_first, post_first)
    up_both = project_rows(normed(after_first, ffn_pre).astype(jnp.bfloat16), (w_gate, w_value))
    hidden_width = w_gate.shape[1]
    up_gate = up_both[:, :hidden_width]
    up_value = up_both[:, hidden_width:]
    rim_gate, rim_value = shifted((up_gate[-2:], up_value[-2:]), "sp", 1)
    gated = (
        jax.nn.gelu(causal_mix(rim_gate, up_gate, conv_gate), approximate=True)
        * causal_mix(rim_value, up_value, conv_value)
    ).astype(jnp.bfloat16)
    ffn_sum = summed_rows(gated, w_down)
    after_ffn = after_first + normed(ffn_sum, ffn_post)
    return attention_layer(after_ffn, pre_second, query_second, 1, out_second, post_second)


def solution(mesh):
    placed = (
        P(("grp", "sp", "tp"), None),
        P(("grp", "sp", "tp"), None),
        P(),
        P(),
        P(None, "tp"),
        P(None, "tp"),
        P("tp", None),
        P(),
        P(),
        P(None, "tp"),
        P(None, "tp"),
        P(None, "tp"),
        P(None, "tp"),
        P("tp", None),
        P(),
        P(),
        P(None, "tp"),
        P(None, "tp"),
        P("tp", None),
        P(),
    )
    return jax.shard_map(
        per_device,
        mesh=mesh,
        in_specs=placed,
        out_specs=P(("grp", "sp", "tp"), None),
        check_vma=False,
    )
```

profile of v0, /device:TPU:23, one launch (start us, length us, event | category | flops | bytes accessed | tf_op | source)
XLA Modules:
  0.0 283.3 jit_solution(5427516378254216936)
XLA Ops:
  6.5 1.7 fusion.8
  8.2 2.5 fusion.10
  10.8 35.0 %all-gather.10.cloned.1.call-done = bf16[1024,2048]{1,0:T(8,128)(2,1)} async-done(((bf16[256,2048]{1,0:T(8,128)(2,1)}), bf16[1024,2048]{1,0:T(8,128)(2,1)}) %all-gather.10.cloned.1.call-update) | async-done | bytes 4194320 | tf_op jit(solution)/shard_map/all_gather | solution.py:52
  45.8 5.2 %fusion.15 = bf16[512,1024]{1,0:T(8,128)(2,1)S(1)} fusion(bf16[1024,2048]{1,0:T(8,128)(2,1)} %all-gather.10.cloned.1.call-done, bf16[2048,256]{1,0:T(8,128)(2,1)} %param.37, bf16[2048,256]{1,0:T(8,128)(2,1)} %param.25), kind=kOutput, calls=%fused_computation.22 | convolution fusion | flops 2152202240 | bytes 7340032 | tf_op jit(solution)/shard_map/rd,dc->cr/dot_general | solution.py:50
  52.9 7.3 %all_gather.24 = bf16[128,2048]{1,0:T(8,128)(2,1)S(1)} all-gather(bf16[32,2048]{1,0:T(8,128)(2,1)S(1)} %fusion.67), channel_id=1, replica_groups=mesh['grp'=2,'sp'=4,'tp'=4] {'tp'}, dimensions={0}, use_global_device_ids=true | all-gather | bytes 655360 | tf_op jit(solution)/shard_map/all_gather | solution.py:31
  60.2 2.1 fusion.24
  62.3 17.4 %all-gather.12.cloned.1.call-done = bf16[1,128,4096]{2,1,0:T(8,128)(2,1)} async-done(((bf16[1,128,1024]{2,1,0:T(8,128)(2,1)}), bf16[1,128,4096]{2,1,0:T(8,128)(2,1)}) %all-gather.12.cloned.1.call-update) | async-done | bytes 1048592 | tf_op jit(solution)/shard_map/all_gather | solution.py:107
  79.7 2.6 multiply_reduce_fusion.1
  82.2 1.5 fusion
  83.7 1.7 copy-done.1
  85.5 23.2 %all-gather.14.cloned.1.call-done = bf16[1,128,4096]{2,1,0:T(8,128)(2,1)} async-done(((bf16[1,128,1024]{2,1,0:T(8,128)(2,1)}), bf16[1,128,4096]{2,1,0:T(8,128)(2,1)}) %all-gather.14.cloned.1.call-update) | async-done | bytes 1048592 | tf_op jit(solution)/shard_map/all_gather | solution.py:108
  108.7 5.5 %fusion.35 = bf16[128,4,128]{0,2,1:T(8,128)(2,1)S(1)} fusion(f32[128,4,4096]{2,0,1:T(8,128)} %copy-done.1, f32[128,4]{0,1:T(4,128)S(1)} %get-tuple-element.19, bf16[1,128,4096]{2,1,0:T(8,128)(2,1)} %all-gather.14.cloned.1.call-done, f32[128,4]{0,1:T(4,128)S(1)} %get-tuple-element.18, f32[128,4]{0,1:T(4,128)S(1)} %get-tuple-element.17), kind=kOutput, calls=%fused_computation.34 | convolution fusion | flops 543358976 | bytes 9574400 | tf_op jit(solution)/shard_map/ths,ds->thd/dot_general | solution.py:85
  115.6 21.1 %reduce-scatter.4.cloned.1.call-done = bf16[32,2048]{1,0:T(8,128)(2,1)} async-done(((bf16[128,2048]{1,0:T(8,128)(2,1)}), bf16[32,2048]{1,0:T(8,128)(2,1)}) %reduce-scatter.4.cloned.1.call-update) | async-done | bytes 131088 | tf_op jit(solution)/shard_map/reduce_scatter | solution.py:40
  140.1 7.8 %all_gather.28 = bf16[128,2048]{1,0:T(8,128)(2,1)S(1)} all-gather(bf16[32,2048]{1,0:T(8,128)(2,1)S(1)} %multiply_convert_fusion.1), channel_id=1, replica_groups=mesh['grp'=2,'sp'=4,'tp'=4] {'tp'}, dimensions={0}, use_global_device_ids=true | all-gather | bytes 655360 | tf_op jit(solution)/shard_map/all_gather | solution.py:31
  147.9 2.7 convolution_convert_fusion.4
  150.8 3.1 %collective-permute-start = (bf16[2,704]{0,1:T(8,128)(2,1)S(1)}, bf16[2,704]{0,1:T(8,128)(2,1)S(1)}, u32[]{:S(2)}, u32[]{:S(2)}) collective-permute-start(bf16[2,704]{0,1:T(8,128)(2,1)S(1)} %slice.80), channel_id=1, source_target_pairs={{0,4},{4,8},{8,12},{1,5},{5,9},{9,13},{2,6},{6,10},{10,14},{3,7},{... | collective-permute-start | bytes 8456 | tf_op jit(solution)/shard_map/ppermute | solution.py:22
  155.0 2.1 collective-permute-start.1
  157.1 1.5 collective-permute-done
  158.8 3.8 %collective-permute-done.1 = bf16[2,704]{0,1:T(8,128)(2,1)S(1)} collective-permute-done((bf16[2,704]{0,1:T(8,128)(2,1)S(1)}, bf16[2,704]{0,1:T(8,128)(2,1)S(1)}, u32[]{:S(2)}, u32[]{:S(2)}) %collective-permute-start.1) | collective-permute-done | bytes 2848 | tf_op jit(solution)/shard_map/ppermute | solution.py:22
  162.7 2.5 convolution_convert_fusion.1
  166.6 20.5 %reduce-scatter.6.cloned.1.call-done = bf16[32,2048]{1,0:T(8,128)(2,1)} async-done(((bf16[128,2048]{1,0:T(8,128)(2,1)}), bf16[32,2048]{1,0:T(8,128)(2,1)}) %reduce-scatter.6.cloned.1.call-update) | async-done | bytes 131088 | tf_op jit(solution)/shard_map/reduce_scatter | solution.py:40
  190.5 7.8 %all_gather.29 = bf16[128,2048]{1,0:T(8,128)(2,1)S(1)} all-gather(bf16[32,2048]{1,0:T(8,128)(2,1)S(1)} %multiply_convert_fusion), channel_id=1, replica_groups=mesh['grp'=2,'sp'=4,'tp'=4] {'tp'}, dimensions={0}, use_global_device_ids=true | all-gather | bytes 655360 | tf_op jit(solution)/shard_map/all_gather | solution.py:31
  198.3 2.0 fusion.25
  200.4 16.2 %all-gather.16.cloned.1.call-done = bf16[1,128,4096]{2,1,0:T(8,128)(2,1)} async-done(((bf16[1,128,1024]{2,1,0:T(8,128)(2,1)}), bf16[1,128,4096]{2,1,0:T(8,128)(2,1)}) %all-gather.16.cloned.1.call-update) | async-done | bytes 1048592 | tf_op jit(solution)/shard_map/all_gather | solution.py:107
  216.6 2.6 multiply_reduce_fusion
  219.2 1.5 fusion.2
  220.7 1.7 copy-done.2
  222.4 23.2 %all-gather.18.cloned.1.call-done = bf16[1,128,4096]{2,1,0:T(8,128)(2,1)} async-done(((bf16[1,128,1024]{2,1,0:T(8,128)(2,1)}), bf16[1,128,4096]{2,1,0:T(8,128)(2,1)}) %all-gather.18.cloned.1.call-update) | async-done | bytes 1048592 | tf_op jit(solution)/shard_map/all_gather | solution.py:108
  245.6 5.5 %fusion.29 = bf16[128,4,128]{0,2,1:T(8,128)(2,1)S(1)} fusion(f32[128,4,4096]{2,0,1:T(8,128)} %copy-done.2, f32[128,4]{0,1:T(4,128)S(1)} %get-tuple-element.21, bf16[1,128,4096]{2,1,0:T(8,128)(2,1)} %all-gather.18.cloned.1.call-done, f32[128,4]{0,1:T(4,128)S(1)} %get-tuple-element.16, f32[128,4]{0,1:T(4,128)S(1)} %get-tuple-element.15), kind=kOutput, calls=%fused_computation.32 | convolution fusion | flops 543358976 | bytes 9574400 | tf_op jit(solution)/shard_map/ths,ds->thd/dot_general | solution.py:85
  251.1 1.3 convolution_convert_fusion
  252.4 21.2 %reduce-scatter.8.cloned.1.call-done = bf16[32,2048]{1,0:T(8,128)(2,1)} async-done(((bf16[128,2048]{1,0:T(8,128)(2,1)}), bf16[32,2048]{1,0:T(8,128)(2,1)}) %reduce-scatter.8.cloned.1.call-update) | async-done | bytes 131088 | tf_op jit(solution)/shard_map/reduce_scatter | solution.py:40
  274.6 1.8 fusion.64
  (74 shorter events, 13.9 us)
Async XLA Ops:
  6.5 156.2 %copy-start = (bf16[704,2048]{1,0:T(8,128)(2,1)S(1)}, bf16[704,2048]{1,0:T(8,128)(2,1)}, u32[]{:S(2)}) copy-start(bf16[704,2048]{1,0:T(8,128)(2,1)} %param.33) | copy-start | bytes 8650756
  6.5 39.3 %all-gather.10.cloned.1.call-start = ((), (), s32[]{:S(2)}) async-start(), calls=%async_computation.3 | async-start | bytes 5242880 | tf_op jit(solution)/shard_map/all_gather | solution.py:52
  10.7 41.4 %copy-start.3 = (bf16[32,2048]{1,0:T(8,128)(2,1)S(1)}, bf16[32,2048]{1,0:T(8,128)(2,1)}, u32[]{:S(2)}) copy-start(bf16[32,2048]{1,0:T(8,128)(2,1)} %param.20) | copy-start | bytes 393220
  10.8 41.5 %copy-start.13 = (f32[2048]{0:T(1024)S(1)}, f32[2048]{0:T(1024)}, u32[]{:S(2)}) copy-start(f32[2048]{0:T(1024)} %param.23) | copy-start | bytes 24580
  10.8 68.9 %all-gather.12.cloned.1.call-start = ((), (), s32[]{:S(2)}) async-start(), calls=%async_computation.7 | async-start | bytes 1310720 | tf_op jit(solution)/shard_map/all_gather | solution.py:107
  52.1 56.5 %all-gather.14.cloned.1.call-start = ((), (), s32[]{:S(2)}) async-start(), calls=%async_computation.8 | async-start | bytes 1310720 | tf_op jit(solution)/shard_map/all_gather | solution.py:108
  52.8 83.8 %reduce-scatter.4.cloned.1.call-start = ((), (), s32[]{:S(2)}) async-start(), calls=%async_computation.4 | async-start | bytes 655360 | tf_op jit(solution)/shard_map/reduce_scatter | solution.py:40
  82.2 3.2 %copy-start.1 = (f32[128,4,4096]{2,0,1:T(8,128)}, f32[128,4,4096]{2,0,1:T(8,128)S(1)}, u32[]{:S(2)}) copy-start(f32[128,4,4096]{2,0,1:T(8,128)S(1)} %get-tuple-element.20) | copy-start | bytes 25165828
  108.6 5.5 %copy-start.6 = (bf16[512,2048]{1,0:T(8,128)(2,1)S(1)}, bf16[512,2048]{1,0:T(8,128)(2,1)}, u32[]{:S(2)}) copy-start(bf16[512,2048]{1,0:T(8,128)(2,1)} %param.26) | copy-start | bytes 6291460
  108.6 6.9 %copy-start.15 = (f32[3,704]{1,0:T(4,128)S(1)}, f32[3,704]{1,0:T(4,128)}, u32[]{:S(2)}) copy-start(f32[3,704]{1,0:T(4,128)} %param.32) | copy-start | bytes 25348
  108.6 6.9 %copy-start.16 = (f32[3,704]{1,0:T(4,128)S(1)}, f32[3,704]{1,0:T(4,128)}, u32[]{:S(2)}) copy-start(f32[3,704]{1,0:T(4,128)} %param.31) | copy-start | bytes 25348
  108.6 29.2 %copy-start.9 = (f32[2048]{0:T(1024)S(1)}, f32[2048]{0:T(1024)}, u32[]{:S(2)}) copy-start(f32[2048]{0:T(1024)} %param.27) | copy-start | bytes 24580
  108.6 30.4 %copy-start.14 = (f32[2048]{0:T(1024)S(1)}, f32[2048]{0:T(1024)}, u32[]{:S(2)}) copy-start(f32[2048]{0:T(1024)} %param.28) | copy-start | bytes 24580
  115.5 71.7 %reduce-scatter.6.cloned.1.call-start = ((), (), s32[]{:S(2)}) async-start(), calls=%async_computation.5 | async-start | bytes 655360 | tf_op jit(solution)/shard_map/reduce_scatter | solution.py:40
  136.7 17.2 %copy-start.5 = (bf16[2048,704]{0,1:T(8,128)(2,1)S(1)}, bf16[2048,704]{0,1:T(8,128)(2,1)}, u32[]{:S(2)}) copy-start(bf16[2048,704]{0,1:T(8,128)(2,1)} %param.30) | copy-start | bytes 8650756
  150.8 7.8 %collective-permute-start = (bf16[2,704]{0,1:T(8,128)(2,1)S(1)}, bf16[2,704]{0,1:T(8,128)(2,1)S(1)}, u32[]{:S(2)}, u32[]{:S(2)}) collective-permute-start(bf16[2,704]{0,1:T(8,128)(2,1)S(1)} %slice.80), channel_id=1, source_target_pairs={{0,4},{4,8},{8,12},{1,5},{5,9},{9,13},{2,6},{6,10},{10,14},{3,7},{... | collective-permute-start | bytes 8456 | tf_op jit(solution)/shard_map/ppermute | solution.py:22
  154.8 33.4 %copy-start.4 = (bf16[32,2048]{1,0:T(8,128)(2,1)S(1)}, bf16[32,2048]{1,0:T(8,128)(2,1)}, u32[]{:S(2)}) copy-start(bf16[32,2048]{1,0:T(8,128)(2,1)} %reduce-scatter.4.cloned.1.call-done) | copy-start | bytes 393220
  154.8 33.4 %copy-start.10 = (f32[2048]{0:T(1024)S(1)}, f32[2048]{0:T(1024)}, u32[]{:S(2)}) copy-start(f32[2048]{0:T(1024)} %param.34) | copy-start | bytes 24580
  154.8 34.6 %copy-start.11 = (f32[2048]{0:T(1024)S(1)}, f32[2048]{0:T(1024)}, u32[]{:S(2)}) copy-start(f32[2048]{0:T(1024)} %param.35) | copy-start | bytes 24580
  155.0 7.6 %collective-permute-start.1 = (bf16[2,704]{0,1:T(8,128)(2,1)S(1)}, bf16[2,704]{0,1:T(8,128)(2,1)S(1)}, u32[]{:S(2)}, u32[]{:S(2)}) collective-permute-start(bf16[2,704]{0,1:T(8,128)(2,1)S(1)} %slice.84), channel_id=1, source_target_pairs={{0,4},{4,8},{8,12},{1,5},{5,9},{9,13},{2,6},{6,10},{10,14},{3,7},{... | collective-permute-start | bytes 8456 | tf_op jit(solution)/shard_map/ppermute | solution.py:22
  165.2 51.4 %all-gather.16.cloned.1.call-start = ((), (), s32[]{:S(2)}) async-start(), calls=%async_computation.9 | async-start | bytes 1310720 | tf_op jit(solution)/shard_map/all_gather | solution.py:107
  165.8 79.7 %all-gather.18.cloned.1.call-start = ((), (), s32[]{:S(2)}) async-start(), calls=%async_computation.10 | async-start | bytes 1310720 | tf_op jit(solution)/shard_map/all_gather | solution.py:108
  166.6 107.0 %reduce-scatter.8.cloned.1.call-start = ((), (), s32[]{:S(2)}) async-start(), calls=%async_computation.6 | async-start | bytes 655360 | tf_op jit(solution)/shard_map/reduce_scatter | solution.py:40
  219.2 3.2 %copy-start.2 = (f32[128,4,4096]{2,0,1:T(8,128)}, f32[128,4,4096]{2,0,1:T(8,128)S(1)}, u32[]{:S(2)}) copy-start(f32[128,4,4096]{2,0,1:T(8,128)S(1)} %get-tuple-element.22) | copy-start | bytes 25165828
  245.6 5.5 %copy-start.7 = (bf16[512,2048]{1,0:T(8,128)(2,1)S(1)}, bf16[512,2048]{1,0:T(8,128)(2,1)}, u32[]{:S(2)}) copy-start(bf16[512,2048]{1,0:T(8,128)(2,1)} %param.38) | copy-start | bytes 6291460
  245.6 29.0 %copy-start.8 = (bf16[32,2048]{1,0:T(8,128)(2,1)S(1)}, bf16[32,2048]{1,0:T(8,128)(2,1)}, u32[]{:S(2)}) copy-start(bf16[32,2048]{1,0:T(8,128)(2,1)} %reduce-scatter.6.cloned.1.call-done) | copy-start | bytes 393220
  245.6 29.0 %copy-start.12 = (f32[2048]{0:T(1024)S(1)}, f32[2048]{0:T(1024)}, u32[]{:S(2)}) copy-start(f32[2048]{0:T(1024)} %param.39) | copy-start | bytes 24580
Sparse Core Ops, SparseCore 0:
  10.9 34.9 all-gather.9
  52.2 27.4 all-gather.11
  81.2 27.3 all-gather.13
  115.6 21.0 reduce-scatter.3
  165.4 21.7 reduce-scatter.5
  188.6 27.9 all-gather.15
  218.2 27.3 all-gather.17
  252.5 20.9 reduce-scatter.7
where the time goes:
time: 287 us; the launch traced here: 283 us
  waiting for transfers between devices  185 us (64%)
  matrix products  34.2 us (12%)
  blocking collectives  22.9 us (8%)
  other arithmetic  17.4 us (6%)
  between operations  13.8 us (5%)
  starting transfers between devices  5.51 us (2%)
  local copies, waits for them, and re-layouts  4.78 us (2%)
    reduce_scatter x3, waiting for transfers between devices, summed_rows(): lax.psum_scatter(jnp.dot(parts, weight, preferred_element_type=jnp.float3...  62.7 us
    all_gather x2, waiting for transfers between devices, attend_keys(): lax.all_gather(values_t, 'sp', axis=1, tiled=True)  46.3 us
    all_gather x1, waiting for transfers between devices, key_columns(): lax.all_gather(source_rows, 'tp', axis=0, tiled=True)  35 us
    all_gather x2, waiting for transfers between devices, attend_keys(): lax.all_gather(keys_t, 'sp', axis=1, tiled=True)  33.6 us
    all_gather x3, blocking collectives, project_rows(): shard_rows = lax.all_gather(rows_here, 'tp', axis=0, tiled=True)  22.9 us
    dot_general x2, matrix products, absorber(): jnp.einsum('ths,ds->thd', weights.astype(jnp.bfloat16), value_block, pref...  11 us
    dot_general x4, matrix products, project_rows(): jnp.dot(shard_rows, weight, preferred_element_type=jnp.float32)  7.78 us
    reduce_sum x7, other arithmetic, normed(): jnp.mean(widened * widened, axis=-1, keepdims=True) + 1e-06  7.38 us
  transfers between devices with their start and end apart: 10, of which 10 were waited for; matrix products, arithmetic and copies ran while one was open for 6% of the time, Pallas kernels for 0%

commit v1 on v0

v1 whole, which is shorter than its diff:
```python
import math

import jax
import jax.numpy as jnp
from jax import lax
from jax.experimental import pallas as pl
from jax.experimental.pallas import tpu as pltpu
from jax.sharding import PartitionSpec as P

HEAD = 128
CHUNKS = 4
EXP_SCALE = HEAD ** (-0.5) * math.log2(math.e)
F32, BF16 = jnp.float32, jnp.bfloat16
MESH = pl.DeviceIdType.MESH


def normed(values, gain):
    widened = values.astype(F32)
    return widened * lax.rsqrt(jnp.mean(widened * widened, axis=-1, keepdims=True) + 1e-06) * gain


def times(start, stop, body):
    if stop - start <= 4:
        for index in range(start, stop):
            body(index)
    else:

        @pl.loop(start, stop)
        def _(index):
            body(index)


def dot(left, right):
    return jnp.dot(left, right, preferred_element_type=F32)


def decoder_kernel(
    n_tp,
    n_sp,
    target_h,
    source_h,
    source_gain,
    pre_first,
    query_first_h,
    keyval_first_h,
    out_first_h,
    post_first,
    ffn_pre,
    gate_h,
    value_h,
    conv_gate,
    conv_value,
    down_h,
    ffn_post,
    pre_second,
    query_second_h,
    keyval_second_h,
    out_second_h,
    post_second,
    decoded,
    target_v,
    source_v,
    query_first,
    keyval_first,
    out_first,
    w_gate,
    w_value,
    w_down,
    query_second,
    keyval_second,
    out_second,
    local_sem,
    hidden,
    hidden_sem,
    src,
    src_send,
    src_recv,
    q_slots,
    q_sem,
    k_first,
    v_first,
    k_second,
    v_second,
    kv_send,
    kv_recv,
    run_max,
    run_sum,
    run_out,
    mix_send,
    mix_recv,
    stat_send,
    stat_recv,
    mix_sem,
    part,
    part_recv,
    part_sem,
    halo_send,
    halo_recv,
    halo_sem,
    stream,
):
    me = lax.axis_index("tp")
    z = lax.axis_index("sp")
    sib = me + 1 - 2 * lax.rem(me, 2)
    n_chip = n_tp // 2
    rows = target_v.shape[0]
    width = target_v.shape[1]
    chunk = src.shape[2]
    block_rows = rows * n_tp

    def tp_at(distance):
        return lax.rem(me + distance, n_tp)

    def sp_at(distance):
        return lax.rem(z + distance, n_sp)

    def to_tp(source, dest, send, recv, device):
        return pltpu.make_async_remote_copy(
            src_ref=source, dst_ref=dest, send_sem=send, recv_sem=recv,
            device_id={"tp": device}, device_id_type=MESH,
        )

    def to_sp(source, dest, send, recv, device):
        return pltpu.make_async_remote_copy(
            src_ref=source, dst_ref=dest, send_sem=send, recv_sem=recv,
            device_id={"sp": device}, device_id_type=MESH,
        )

    pairs = [
        (target_h, target_v),
        (source_h, source_v),
        (query_first_h, query_first),
        (keyval_first_h, keyval_first),
        (keyval_second_h, keyval_second),
        (out_first_h, out_first),
        (gate_h, w_gate),
        (value_h, w_value),
        (down_h, w_down),
        (query_second_h, query_second),
        (out_second_h, out_second),
    ]
    loads = [
        pltpu.make_async_copy(a, b, local_sem.at[i]) for i, (a, b) in enumerate(pairs)
    ]
    for load in loads:
        load.start()

    barrier = pltpu.get_barrier_semaphore()
    for distance in range(1, n_tp):
        pl.semaphore_signal(barrier, inc=1, device_id={"tp": tp_at(distance)}, device_id_type=MESH)
    for distance in range(1, n_sp):
        pl.semaphore_signal(barrier, inc=1, device_id={"sp": sp_at(distance)}, device_id_type=MESH)
    pl.semaphore_wait(barrier, n_tp - 1 + n_sp - 1)

    def hidden_copy(phase, slot, device):
        return to_tp(
            hidden.at[phase, slot], hidden.at[phase, slot],
            hidden_sem.at[0, phase, 0], hidden_sem.at[1, phase, slot], device,
        )

    def gather_start(phase, value):
        hidden[phase, me] = value.astype(BF16)
        for d in range(1, n_chip):
            hidden_copy(phase, me, tp_at(2 * d)).start()
        hidden_copy(phase, me, sib).start()

    def gather_finish(phase):
        for d in range(1, n_chip):
            slot = tp_at(2 * d)
            hidden_copy(phase, slot, sib).wait_recv()
            hidden_copy(phase, slot, sib).start()
        hidden_copy(phase, sib, sib).wait_recv()
        for d in range(1, n_chip):
            hidden_copy(phase, lax.rem(sib + 2 * d, n_tp), sib).wait_recv()
        whole = hidden[phase]
        if rows % 16:
            return whole.astype(F32).reshape(block_rows, width).astype(BF16)
        return whole.reshape(block_rows, width)

    def gather_drain(phase):
        for _ in range(2 * n_chip - 1):
            hidden_copy(phase, me, sib).wait_send()

    def part_copy(phase, distance, slot):
        return to_tp(
            part.at[phase, tp_at(distance)], part_recv.at[phase, slot],
            part_sem.at[0, phase, 0], part_sem.at[1, phase, slot], tp_at(distance),
        )

    def scatter_sum(phase, product):
        part[phase] = product.reshape(n_tp, rows, width).astype(BF16)
        order = [d for d in range(1, n_tp) if d != 2] + ([2] if n_tp > 2 else [])
        for d in order:
            part_copy(phase, d, me).start()
        total = part[phase, me].astype(F32)
        for d in range(1, n_tp):
            slot = tp_at(d)
            part_copy(phase, d, slot).wait_recv()
            total = total + part_recv[phase, slot].astype(F32)
        for d in range(1, n_tp):
            part_copy(phase, d, me).wait_send()
        return total

    def head_columns(queries):
        blocks = [
            queries[:, h : h + HEAD].T for h in range(0, queries.shape[1], HEAD)
        ]
        return jnp.concatenate(blocks, axis=1).astype(BF16)

    def head_rows(columns):
        blocks = [
            columns[:, c : c + block_rows].T for c in range(0, columns.shape[1], block_rows)
        ]
        return jnp.concatenate(blocks, axis=1).astype(BF16)

    loads[0].wait()
    gather_start(0, normed(target_v[...], pre_first[...]))

    def src_copy(slot, c, device, kind):
        return to_tp(
            src.at[slot, c], src.at[slot, c], src_send.at[kind], src_recv.at[slot, c], device
        )

    loads[1].wait()
    for c in range(CHUNKS):
        src[me, c] = normed(source_v[pl.ds(c * chunk, chunk)], source_gain[...]).astype(BF16)
        for d in range(1, n_chip):
            src_copy(me, c, tp_at(2 * d), 0).start()
        src_copy(me, c, sib, 0).start()

    loads[2].wait()
    q_slots[z] = head_columns(dot(gather_finish(0), query_first[...]))

    def q_copy(distance, slot):
        return to_sp(
            q_slots.at[z], q_slots.at[z] if slot is None else q_slots.at[slot],
            q_sem.at[0, 0], q_sem.at[1, z if slot is None else slot], sp_at(distance),
        )

    for d in range(1, n_sp):
        q_copy(d, None).start()

    loads[3].wait()
    loads[4].wait()

    def project(lines, block, offset):
        first = dot(lines, keyval_first[...])
        second = dot(lines, keyval_second[...])
        span = pl.ds(offset, lines.shape[0])
        k_first[block, span] = first[:, :HEAD].astype(BF16)
        v_first[block, span] = first[:, HEAD:].astype(BF16)
        k_second[z, block, span] = second[:, :HEAD].astype(BF16)
        v_second[z, block, span] = second[:, HEAD:].astype(BF16)

    def project_pair(block, c, mine, other):
        lines = jnp.concatenate([src[mine, c], src[other, c]], axis=0)
        project(lines, block, c * 2 * chunk)

    def absorb(keys, values, queries, slot, fresh):
        scores = dot(keys, queries)
        newest = jnp.max(scores, axis=0, keepdims=True)
        if not fresh:
            newest = jnp.maximum(newest, run_max[slot])
        weights = jnp.exp2((scores - newest) * EXP_SCALE)
        added = jnp.sum(weights, axis=0, keepdims=True)
        gathered = lax.dot_general(
            values, weights.astype(BF16), (((0,), (0,)), ((), ())), preferred_element_type=F32
        )
        if not fresh:
            rescale = jnp.exp2((run_max[slot] - newest) * EXP_SCALE)
            added = added + run_sum[slot] * rescale
            gathered = gathered + run_out[slot] * rescale
        run_max[slot] = newest
        run_sum[slot] = added
        run_out[slot] = gathered

    def absorb_block(block, fresh):
        @pl.loop(0, n_sp)
        def _(slot):
            absorb(k_first[block], v_first[block], q_slots[slot], slot, fresh)

    def kv_copies(block, slot, distance):
        peer = sp_at(distance)
        return [
            to_sp(
                store.at[z, block], store.at[slot, block],
                kv_send.at[index], kv_recv.at[index, slot, block], peer,
            )
            for index, store in enumerate((k_second, v_second))
        ]

    def kv_start(block):
        def one(d):
            for copy in kv_copies(block, z, d):
                copy.start()

        times(1, n_sp, one)

    for c in range(CHUNKS):
        src_copy(sib, c, sib, 0).wait_recv()
        project_pair(0, c, me, sib)
    for d in range(1, n_sp):
        q_copy(d, sp_at(d)).wait_recv()
    kv_start(0)
    absorb_block(0, True)

    def far_chip(d):
        near = tp_at(2 * d)
        far = lax.rem(sib + 2 * d, n_tp)
        for c in range(CHUNKS):
            src_copy(near, c, sib, 1).wait_recv()
            src_copy(near, c, sib, 1).start()
            src_copy(far, c, sib, 1).wait_recv()
            project_pair(d, c, near, far)
        absorb_block(d, False)

    times(1, n_chip, far_chip)

    def mix_copies(distance, slot):
        peer = sp_at(distance)
        return [
            to_sp(sent.at[peer], got.at[slot], mix_sem.at[index, 0, 0], mix_sem.at[index, 1, slot], peer)
            for index, (sent, got) in enumerate(((mix_send, mix_recv), (stat_send, stat_recv)))
        ]

    @pl.loop(0, n_sp)
    def _(slot):
        total = run_sum[slot]
        mix_send[slot] = (run_out[slot] / total).astype(BF16)
        stat_send[slot] = jnp.concatenate([run_max[slot], total], axis=0)

    for d in range(1, n_sp):
        for copy in mix_copies(d, z):
            copy.start()
    for d in range(1, n_sp):
        for copy in mix_copies(d, sp_at(d)):
            copy.wait_recv()
    for block in range(1, n_chip):
        kv_start(block)
    mix_recv[z] = mix_send[z]
    stat_recv[z] = stat_send[z]
    top = stat_recv[0, 0:1]
    for slot in range(1, n_sp):
        top = jnp.maximum(top, stat_recv[slot, 0:1])
    weight_sum = jnp.zeros_like(top)
    weighted = jnp.zeros(run_out.shape[1:], F32)
    for slot in range(n_sp):
        share = jnp.exp2((stat_recv[slot, 0:1] - top) * EXP_SCALE) * stat_recv[slot, 1:2]
        weight_sum = weight_sum + share
        weighted = weighted + mix_recv[slot].astype(F32) * share
    loads[5].wait()
    mixed = scatter_sum(0, dot(head_rows(weighted / weight_sum), out_first[...]))
    after_first = target_v[...].astype(F32) + normed(mixed, post_first[...])
    stream[...] = after_first

    gather_start(1, normed(after_first, ffn_pre[...]))
    loads[6].wait()
    loads[7].wait()
    ffn_input = gather_finish(1)
    up_gate = dot(ffn_input, w_gate[...]).astype(BF16)
    up_value = dot(ffn_input, w_value[...]).astype(BF16)
    halo_send[0] = up_gate[block_rows - 16 :]
    halo_send[1] = up_value[block_rows - 16 :]
    halo = to_sp(halo_send, halo_recv, halo_sem.at[0], halo_sem.at[1], sp_at(1))

    @pl.when(z < n_sp - 1)
    def _():
        halo.start()

    @pl.when(z > 0)
    def _():
        halo.wait_recv()

    def causal_mix(up_rows, rim, taps):
        here = up_rows.astype(F32)
        rim = jnp.where(z > 0, rim.astype(F32), 0.0)
        row = lax.broadcasted_iota(jnp.int32, here.shape, 0)
        before = jnp.where(row == 0, rim[15:16], pltpu.roll(here, 1, 0))
        earlier = jnp.where(
            row == 0, rim[14:15], jnp.where(row == 1, rim[15:16], pltpu.roll(here, 2, 0))
        )
        return taps[0:1] * earlier + taps[1:2] * before + taps[2:3] * here

    gated = (
        jax.nn.gelu(causal_mix(up_gate, halo_recv[0], conv_gate[...]), approximate=True)
        * causal_mix(up_value, halo_recv[1], conv_value[...])
    ).astype(BF16)
    loads[8].wait()
    ffn_sum = scatter_sum(1, dot(gated, w_down[...]))
    after_ffn = stream[...] + normed(ffn_sum, ffn_post[...])
    stream[...] = after_ffn

    gather_start(2, normed(after_ffn, pre_second[...]))
    loads[9].wait()
    queries = head_columns(dot(gather_finish(2), query_second[...]))
    for d in range(1, n_sp):
        q_copy(d, None).wait_send()
    q_slots[z] = queries

    for block in range(n_chip):
        absorb(k_second[z, block], v_second[z, block], q_slots[z], 0, block == 0)

    def absorb_slot(d):
        slot = sp_at(d)
        for block in range(n_chip):
            for copy in kv_copies(block, slot, d):
                copy.wait_recv()
            absorb(k_second[slot, block], v_second[slot, block], q_slots[z], 0, False)

    times(1, n_sp, absorb_slot)
    loads[10].wait()
    mixed = scatter_sum(2, dot(head_rows(run_out[0] / run_sum[0]), out_second[...]))
    decoded[...] = stream[...] + normed(mixed, post_second[...])

    for phase in range(3):
        gather_drain(phase)
    for c in range(CHUNKS):
        for _ in range(n_chip):
            src_copy(me, c, sib, 0).wait_send()
        for d in range(1, n_chip):
            src_copy(me, c, sib, 1).wait_send()

    def drain(d):
        for block in range(n_chip):
            for copy in kv_copies(block, z, d):
                copy.wait_send()
        for copy in mix_copies(d, z):
            copy.wait_send()

    times(1, n_sp, drain)

    @pl.when(z < n_sp - 1)
    def _():
        halo.wait_send()


def per_device(*arrays):
    (target, source, source_gain, pre_first, query_first, keyval_first, out_first, post_first,
     ffn_pre, w_gate, w_value, conv_gate, conv_value, w_down, ffn_post, pre_second,
     query_second, keyval_second, out_second, post_second) = arrays
    n_tp, n_sp = lax.axis_size("tp"), lax.axis_size("sp")
    sharers = 2 * HEAD // keyval_first.shape[1]
    if sharers > 1:
        groups = [list(range(low, low + sharers)) for low in range(0, n_tp, sharers)]
        keyval_first, keyval_second = (
            lax.all_gather(w, "tp", axis=1, tiled=True, axis_index_groups=groups)
            for w in (keyval_first, keyval_second)
        )
    rows, width = target.shape
    lines = source.shape[0]
    block_rows = rows * n_tp
    columns = query_first.shape[1] // HEAD * block_rows
    hidden_units = w_gate.shape[1]
    n_chip = n_tp // 2
    dma = pltpu.SemaphoreType.DMA
    any_spec = pl.BlockSpec(memory_space=pl.ANY)
    vmem = pl.BlockSpec(memory_space=pltpu.VMEM)

    def row(gain):
        return gain.reshape(1, width)

    scratch = [
        pltpu.VMEM(target.shape, BF16),
        pltpu.VMEM(source.shape, BF16),
        *(pltpu.VMEM(w.shape, BF16) for w in (
            query_first, keyval_first, out_first, w_gate, w_value, w_down,
            query_second, keyval_second, out_second)),
        dma((11,)),
        pltpu.VMEM((3, n_tp, rows, width), BF16),
        dma((2, 3, n_tp)),
        pltpu.VMEM((n_tp, CHUNKS, lines // CHUNKS, width), BF16),
        dma((2,)),
        dma((n_tp, CHUNKS)),
        pltpu.VMEM((n_sp, HEAD, columns), BF16),
        dma((2, n_sp)),
        pltpu.VMEM((n_chip, 2 * lines, HEAD), BF16),
        pltpu.VMEM((n_chip, 2 * lines, HEAD), BF16),
        pltpu.VMEM((n_sp, n_chip, 2 * lines, HEAD), BF16),
        pltpu.VMEM((n_sp, n_chip, 2 * lines, HEAD), BF16),
        dma((2,)),
        dma((2, n_sp, n_chip)),
        pltpu.VMEM((n_sp, 1, columns), F32),
        pltpu.VMEM((n_sp, 1, columns), F32),
        pltpu.VMEM((n_sp, HEAD, columns), F32),
        pltpu.VMEM((n_sp, HEAD, columns), BF16),
        pltpu.VMEM((n_sp, HEAD, columns), BF16),
        pltpu.VMEM((n_sp, 2, columns), F32),
        pltpu.VMEM((n_sp, 2, columns), F32),
        dma((2, 2, n_sp)),
        pltpu.VMEM((3, n_tp, rows, width), BF16),
        pltpu.VMEM((3, n_tp, rows, width), BF16),
        dma((2, 3, n_tp)),
        pltpu.VMEM((2, 16, hidden_units), BF16),
        pltpu.VMEM((2, 16, hidden_units), BF16),
        dma((2,)),
        pltpu.VMEM((rows, width), F32),
    ]

    def kernel(*refs):
        decoder_kernel(n_tp, n_sp, *refs)

    return pl.pallas_call(
        kernel,
        out_shape=jax.ShapeDtypeStruct((rows, width), F32),
        in_specs=[any_spec, any_spec, vmem, vmem, any_spec, any_spec, any_spec, vmem, vmem,
                  any_spec, any_spec, vmem, vmem, any_spec, vmem, vmem, any_spec, any_spec,
                  any_spec, vmem],
        out_specs=vmem,
        scratch_shapes=scratch,
        compiler_params=pltpu.CompilerParams(
            collective_id=0, has_side_effects=True, vmem_limit_bytes=67_000_000
        ),
        name="decoder",
    )(
        target, source, row(source_gain), row(pre_first), query_first, keyval_first, out_first,
        row(post_first), row(ffn_pre), w_gate, w_value, conv_gate, conv_value, w_down,
        row(ffn_post), row(pre_second), query_second, keyval_second, out_second, row(post_second),
    )


def solution(mesh):
    rows = P(("grp", "sp", "tp"), None)
    by_column, by_row = P(None, "tp"), P("tp", None)
    placed = (
        rows, rows, P(), P(), by_column, by_column, by_row, P(), P(), by_column, by_column,
        by_column, by_column, by_row, P(), P(), by_column, by_column, by_row, P(),
    )
    return jax.shard_map(
        per_device, mesh=mesh, in_specs=placed, out_specs=rows, check_vma=False
    )
```

time: 287 us -> 121 us (0.42); the launches traced: 283 us -> 121 us
  waiting for transfers between devices: 185 us -> 0 us
  Pallas kernels: 0 us -> 112 us
  matrix products: 34.2 us -> 0 us
  blocking collectives: 22.9 us -> 0 us
  other arithmetic: 17.4 us -> 0 us
  between operations: 13.8 us -> 0.01 us
  starting transfers between devices: 5.51 us -> 0 us
  local copies, waits for them, and re-layouts: 4.78 us -> 9.25 us
    all_gather x5 -> x0, waiting for transfers between devices: 115 us -> none  [the longest x2 46.3 us: attend_keys(): lax.all_gather(values_t, 'sp', axis=1, tiled=True)]
    pallas_call x0 -> x1, Pallas kernels: none -> 112 us  [per_device(): pl.pallas_call(kernel, out_shape=jax.ShapeDtypeStruct((rows, width), F32)...]
    reduce_scatter x3 -> x0, waiting for transfers between devices: 62.7 us -> none  [summed_rows(): lax.psum_scatter(jnp.dot(parts, weight, preferred_element_type=jnp.float3...]
    dot_general x12 -> x0, matrix products: 34.2 us -> none  [the longest x2 11 us: absorber(): jnp.einsum('ths,ds->thd', weights.astype(jnp.bfloat16), value_block, pref...]
    all_gather x3 -> x0, blocking collectives: 22.9 us -> none  [project_rows(): shard_rows = lax.all_gather(rows_here, 'tp', axis=0, tiled=True)]
    reduce_sum x9 -> x0, other arithmetic: 10.4 us -> none  [the longest x7 7.38 us: normed(): jnp.mean(widened * widened, axis=-1, keepdims=True) + 1e-06]
    unnamed x34 -> x5, local copies, waits for them, and re-layouts: 3.51 us -> 9.25 us
    ppermute x2 -> x0, waiting for transfers between devices: 5.28 us -> none  [shifted(): lax.ppermute(value, axis, [(source, source + steps) for source in range(l...]
  transfers between devices with their start and end apart: 10 -> 0, of which waited for: 10 -> 0; matrix products, arithmetic and copies ran while one was open for 6% -> 0% of each run, Pallas kernels for 0% -> 0%
where the time goes in v1:
time: 121 us
  Pallas kernels  112 us (93%)
  local copies, waits for them, and re-layouts  9.25 us (8%)
    pallas_call x1, Pallas kernels, per_device(): pl.pallas_call(kernel, out_shape=jax.ShapeDtypeStruct((rows, width), F32)...  112 us
    unnamed x5, local copies, waits for them, and re-layouts  9.25 us

profile of v1, /device:TPU:23, one launch (start us, length us, event | category | flops | bytes accessed | tf_op | source)
XLA Modules:
  0.0 121.0 jit_solution(15543101037104579261)
XLA Ops:
  0.0 0.0 copy-start
  0.0 4.7 %copy.21.refs_9_ = bf16[2048,704]{1,0:T(8,128)(2,1)} copy(bf16[2048,704]{0,1:T(8,128)(2,1)} %param.29) | data formatting | bytes 5767168 | tf_op args[9]
  4.8 0.0 copy-done
  4.8 2.8 %copy.22.refs_10_ = bf16[2048,704]{1,0:T(8,128)(2,1)} copy(bf16[2048,704]{0,1:T(8,128)(2,1)S(1)} %copy-done) | data formatting | bytes 5767168 | tf_op args[10]
  7.6 111.8 %decoder.1 = f32[32,2048]{1,0:T(8,128)} custom-call(bf16[32,2048]{1,0:T(8,128)(2,1)} %refs_0_.1, bf16[256,2048]{1,0:T(8,128)(2,1)} %refs_1_.1, f32[1,2048]{1,0:T(1,128)} %bitcast.7, f32[1,2048]{1,0:T(1,128)} %bitcast.8, bf16[2048,512]{1,0:T(8,128)(2,1)} %refs_4_.1, bf16[2048,256]{1,0:T(8,128)(2,1)} %refs_5_.1, bf16[512,2048]{1,0:T(8,128)(2,1)} %refs_6_.1, ...), custom_call_target="tpu_custom_call" | custom-call | tf_op jit(solution)/shard_map/decoder/pallas_call | solution.py:502
  119.4 1.7 %copy.24 = f32[32,2048]{1,0:T(8,128)} copy(f32[32,2048]{1,0:T(8,128)} %decoder.1) | data formatting | bytes 524288
Async XLA Ops:
  0.0 4.8 %copy-start = (bf16[2048,704]{0,1:T(8,128)(2,1)S(1)}, bf16[2048,704]{0,1:T(8,128)(2,1)}, u32[]{:S(2)}) copy-start(bf16[2048,704]{0,1:T(8,128)(2,1)} %param.30) | copy-start | bytes 8650756

commit v2 on v1

--- a/solution.py
+++ b/solution.py
@@ -9,6 +9,7 @@
 
 HEAD = 128
 CHUNKS = 4
+PIECES = 2
 EXP_SCALE = HEAD ** (-0.5) * math.log2(math.e)
 F32, BF16 = jnp.float32, jnp.bfloat16
 MESH = pl.DeviceIdType.MESH
@@ -71,7 +72,8 @@
     out_second,
     local_sem,
     hidden,
-    hidden_sem,
+    hidden_send,
+    hidden_recv,
     src,
     src_send,
     src_recv,
@@ -92,7 +94,11 @@
     stat_recv,
     mix_sem,
     part,
+    pair_recv,
+    pair_sum,
     part_recv,
+    part_send,
+    pair_sem,
     part_sem,
     halo_send,
     halo_recv,
@@ -102,9 +108,11 @@
     me = lax.axis_index("tp")
     z = lax.axis_index("sp")
     sib = me + 1 - 2 * lax.rem(me, 2)
+    core, chip = lax.rem(me, 2), me // 2
     n_chip = n_tp // 2
     rows = target_v.shape[0]
     width = target_v.shape[1]
+    span = width // PIECES
     chunk = src.shape[2]
     block_rows = rows * n_tp
 
@@ -152,54 +160,89 @@
         pl.semaphore_signal(barrier, inc=1, device_id={"sp": sp_at(distance)}, device_id_type=MESH)
     pl.semaphore_wait(barrier, n_tp - 1 + n_sp - 1)
 
-    def hidden_copy(phase, slot, device):
+    def hidden_copy(phase, piece, slot, device):
         return to_tp(
-            hidden.at[phase, slot], hidden.at[phase, slot],
-            hidden_sem.at[0, phase, 0], hidden_sem.at[1, phase, slot], device,
+            hidden.at[phase, piece, slot], hidden.at[phase, piece, slot],
+            hidden_send.at[phase], hidden_recv.at[phase, piece, slot], device,
         )
 
     def gather_start(phase, value):
-        hidden[phase, me] = value.astype(BF16)
-        for d in range(1, n_chip):
-            hidden_copy(phase, me, tp_at(2 * d)).start()
-        hidden_copy(phase, me, sib).start()
-
-    def gather_finish(phase):
-        for d in range(1, n_chip):
-            slot = tp_at(2 * d)
-            hidden_copy(phase, slot, sib).wait_recv()
-            hidden_copy(phase, slot, sib).start()
-        hidden_copy(phase, sib, sib).wait_recv()
-        for d in range(1, n_chip):
-            hidden_copy(phase, lax.rem(sib + 2 * d, n_tp), sib).wait_recv()
-        whole = hidden[phase]
-        if rows % 16:
-            return whole.astype(F32).reshape(block_rows, width).astype(BF16)
-        return whole.reshape(block_rows, width)
+        for piece in range(PIECES):
+            hidden[phase, piece, me] = value[:, piece * span : (piece + 1) * span].astype(BF16)
+            for d in range(1, n_chip):
+                hidden_copy(phase, piece, me, tp_at(2 * d)).start()
+            hidden_copy(phase, piece, me, sib).start()
+
+    def gather_times(phase, weights):
+        totals = [None] * len(weights)
+        for piece in range(PIECES + 1):
+            if piece < PIECES:
+                for d in range(1, n_chip):
+                    slot = tp_at(2 * d)
+                    hidden_copy(phase, piece, slot, sib).wait_recv()
+                    hidden_copy(phase, piece, slot, sib).start()
+            if piece == 0:
+                continue
+            ready = piece - 1
+            for d in range(n_chip):
+                slot = lax.rem(sib + 2 * d, n_tp)
+                hidden_copy(phase, ready, slot, sib).wait_recv()
+            whole = hidden[phase, ready]
+            if rows % 16:
+                whole = whole.astype(F32).reshape(block_rows, span).astype(BF16)
+            else:
+                whole = whole.reshape(block_rows, span)
+            for index, weight in enumerate(weights):
+                product = dot(whole, weight[ready * span : (ready + 1) * span, :])
+                totals[index] = product if ready == 0 else totals[index] + product
+        return totals
 
     def gather_drain(phase):
-        for _ in range(2 * n_chip - 1):
-            hidden_copy(phase, me, sib).wait_send()
-
-    def part_copy(phase, distance, slot):
+        for piece in range(PIECES):
+            for _ in range(2 * n_chip - 1):
+                hidden_copy(phase, piece, me, sib).wait_send()
+
+    def pair_copy(phase, piece):
         return to_tp(
-            part.at[phase, tp_at(distance)], part_recv.at[phase, slot],
-            part_sem.at[0, phase, 0], part_sem.at[1, phase, slot], tp_at(distance),
-        )
-
-    def scatter_sum(phase, product):
-        part[phase] = product.reshape(n_tp, rows, width).astype(BF16)
-        order = [d for d in range(1, n_tp) if d != 2] + ([2] if n_tp > 2 else [])
-        for d in order:
-            part_copy(phase, d, me).start()
-        total = part[phase, me].astype(F32)
-        for d in range(1, n_tp):
-            slot = tp_at(d)
-            part_copy(phase, d, slot).wait_recv()
-            total = total + part_recv[phase, slot].astype(F32)
-        for d in range(1, n_tp):
-            part_copy(phase, d, me).wait_send()
-        return total
+            part.at[phase, piece, 1 - core], pair_recv.at[phase, piece],
+            part_send.at[phase, 0], pair_sem.at[phase, piece], sib,
+        )
+
+    def chip_copy(phase, piece, distance, slot):
+        other = lax.rem(chip + distance, n_chip)
+        return to_tp(
+            pair_sum.at[phase, piece, other], part_recv.at[phase, piece, slot],
+            part_send.at[phase, 1], part_sem.at[phase, piece, slot], 2 * other + core,
+        )
+
+    def scatter_sum(phase, left, weight):
+        for piece in range(PIECES):
+            product = dot(left, weight[:, piece * span : (piece + 1) * span])
+            product = product.reshape(n_chip, 2, rows, span)
+            for parity in range(2):
+                part[phase, piece, parity] = product[:, parity].astype(BF16)
+            pair_copy(phase, piece).start()
+        for piece in range(PIECES):
+            pair_copy(phase, piece).wait_recv()
+            mine = part[phase, piece, core].astype(F32)
+            pair_sum[phase, piece] = (mine + pair_recv[phase, piece].astype(F32)).astype(BF16)
+            for d in range(1, n_chip):
+                chip_copy(phase, piece, d, chip).start()
+        sums = []
+        for piece in range(PIECES):
+            total = pair_sum[phase, piece, chip].astype(F32)
+            for d in range(1, n_chip):
+                slot = lax.rem(chip + d, n_chip)
+                chip_copy(phase, piece, d, slot).wait_recv()
+                total = total + part_recv[phase, piece, slot].astype(F32)
+            sums.append(total)
+        return jnp.concatenate(sums, axis=1)
+
+    def sum_drain(phase):
+        for piece in range(PIECES):
+            pair_copy(phase, piece).wait_send()
+            for d in range(1, n_chip):
+                chip_copy(phase, piece, d, chip).wait_send()
 
     def head_columns(queries):
         blocks = [
@@ -229,7 +272,7 @@
         src_copy(me, c, sib, 0).start()
 
     loads[2].wait()
-    q_slots[z] = head_columns(dot(gather_finish(0), query_first[...]))
+    q_slots[z] = head_columns(gather_times(0, [query_first])[0])
 
     def q_copy(distance, slot):
         return to_sp(
@@ -246,11 +289,11 @@
     def project(lines, block, offset):
         first = dot(lines, keyval_first[...])
         second = dot(lines, keyval_second[...])
-        span = pl.ds(offset, lines.shape[0])
-        k_first[block, span] = first[:, :HEAD].astype(BF16)
-        v_first[block, span] = first[:, HEAD:].astype(BF16)
-        k_second[z, block, span] = second[:, :HEAD].astype(BF16)
-        v_second[z, block, span] = second[:, HEAD:].astype(BF16)
+        place = pl.ds(offset, lines.shape[0])
+        k_first[block, place] = first[:, :HEAD].astype(BF16)
+        v_first[block, place] = first[:, HEAD:].astype(BF16)
+        k_second[z, block, place] = second[:, :HEAD].astype(BF16)
+        v_second[z, block, place] = second[:, HEAD:].astype(BF16)
 
     def project_pair(block, c, mine, other):
         lines = jnp.concatenate([src[mine, c], src[other, c]], axis=0)
@@ -279,29 +322,49 @@
         def _(slot):
             absorb(k_first[block], v_first[block], q_slots[slot], slot, fresh)
 
-    def kv_copies(block, slot, distance):
-        peer = sp_at(distance)
+    def kv_copies(block, slot, peer):
         return [
             to_sp(
-                store.at[z, block], store.at[slot, block],
+                store.at[slot, block], store.at[slot, block],
                 kv_send.at[index], kv_recv.at[index, slot, block], peer,
             )
             for index, store in enumerate((k_second, v_second))
         ]
 
-    def kv_start(block):
-        def one(d):
-            for copy in kv_copies(block, z, d):
-                copy.start()
-
-        times(1, n_sp, one)
+    def kv_hop(block, hop, arrive=True, leave=True):
+        for step in (1, -1):
+            slot = z - step * (hop - 1)
+            peer = z + step
+
+            @pl.when(jnp.logical_and(slot >= 0, slot < n_sp))
+            def _():
+                if arrive:
+                    for copy in kv_copies(block, slot, sp_at(1)):
+                        copy.wait_recv()
+                if leave:
+
+                    @pl.when(jnp.logical_and(hop < n_sp, jnp.logical_and(peer >= 0, peer < n_sp)))
+                    def _():
+                        for copy in kv_copies(block, slot, peer):
+                            copy.start()
+
+    def kv_drain(block, hop):
+        for step in (1, -1):
+            slot = z - step * (hop - 1)
+            peer = z + step
+            inside = jnp.logical_and(slot >= 0, slot < n_sp)
+
+            @pl.when(jnp.logical_and(inside, jnp.logical_and(peer >= 0, peer < n_sp)))
+            def _():
+                for copy in kv_copies(block, slot, peer):
+                    copy.wait_send()
 
     for c in range(CHUNKS):
         src_copy(sib, c, sib, 0).wait_recv()
         project_pair(0, c, me, sib)
     for d in range(1, n_sp):
         q_copy(d, sp_at(d)).wait_recv()
-    kv_start(0)
+    kv_hop(0, 1, arrive=False)
     absorb_block(0, True)
 
     def far_chip(d):
@@ -312,9 +375,14 @@
             src_copy(near, c, sib, 1).start()
             src_copy(far, c, sib, 1).wait_recv()
             project_pair(d, c, near, far)
+
+    def far_absorb(d):
+        far_chip(d)
         absorb_block(d, False)
 
-    times(1, n_chip, far_chip)
+    times(1, n_chip - 1, far_absorb)
+    last = n_chip - 1
+    far_chip(last)
 
     def mix_copies(distance, slot):
         peer = sp_at(distance)
@@ -323,22 +391,25 @@
             for index, (sent, got) in enumerate(((mix_send, mix_recv), (stat_send, stat_recv)))
         ]
 
-    @pl.loop(0, n_sp)
-    def _(slot):
+    def finish_slot(slot, mixes, stats):
+        absorb(k_first[last], v_first[last], q_slots[slot], slot, False)
         total = run_sum[slot]
-        mix_send[slot] = (run_out[slot] / total).astype(BF16)
-        stat_send[slot] = jnp.concatenate([run_max[slot], total], axis=0)
-
-    for d in range(1, n_sp):
+        mixes[slot] = (run_out[slot] / total).astype(BF16)
+        stats[slot] = jnp.concatenate([run_max[slot], total], axis=0)
+
+    @pl.loop(1, n_sp)
+    def _(d):
+        finish_slot(sp_at(d), mix_send, stat_send)
         for copy in mix_copies(d, z):
             copy.start()
+
+    finish_slot(z, mix_recv, stat_recv)
     for d in range(1, n_sp):
         for copy in mix_copies(d, sp_at(d)):
             copy.wait_recv()
+    kv_hop(0, 2)
     for block in range(1, n_chip):
-        kv_start(block)
-    mix_recv[z] = mix_send[z]
-    stat_recv[z] = stat_send[z]
+        kv_hop(block, 1, arrive=False)
     top = stat_recv[0, 0:1]
     for slot in range(1, n_sp):
         top = jnp.maximum(top, stat_recv[slot, 0:1])
@@ -349,16 +420,17 @@
         weight_sum = weight_sum + share
         weighted = weighted + mix_recv[slot].astype(F32) * share
     loads[5].wait()
-    mixed = scatter_sum(0, dot(head_rows(weighted / weight_sum), out_first[...]))
+    mixed = scatter_sum(0, head_rows(weighted / weight_sum), out_first)
     after_first = target_v[...].astype(F32) + normed(mixed, post_first[...])
     stream[...] = after_first
 
     gather_start(1, normed(after_first, ffn_pre[...]))
+    kv_hop(0, 3)
+    for block in range(1, n_chip):
+        kv_hop(block, 2)
     loads[6].wait()
     loads[7].wait()
-    ffn_input = gather_finish(1)
-    up_gate = dot(ffn_input, w_gate[...]).astype(BF16)
-    up_value = dot(ffn_input, w_value[...]).astype(BF16)
+    up_gate, up_value = (up.astype(BF16) for up in gather_times(1, [w_gate, w_value]))
     halo_send[0] = up_gate[block_rows - 16 :]
     halo_send[1] = up_value[block_rows - 16 :]
     halo = to_sp(halo_send, halo_recv, halo_sem.at[0], halo_sem.at[1], sp_at(1))
@@ -386,13 +458,15 @@
         * causal_mix(up_value, halo_recv[1], conv_value[...])
     ).astype(BF16)
     loads[8].wait()
-    ffn_sum = scatter_sum(1, dot(gated, w_down[...]))
+    ffn_sum = scatter_sum(1, gated, w_down)
     after_ffn = stream[...] + normed(ffn_sum, ffn_post[...])
     stream[...] = after_ffn
 
     gather_start(2, normed(after_ffn, pre_second[...]))
+    for block in range(1, n_chip):
+        kv_hop(block, 3)
     loads[9].wait()
-    queries = head_columns(dot(gather_finish(2), query_second[...]))
+    queries = head_columns(gather_times(2, [query_second])[0])
     for d in range(1, n_sp):
         q_copy(d, None).wait_send()
     q_slots[z] = queries
@@ -400,20 +474,24 @@
     for block in range(n_chip):
         absorb(k_second[z, block], v_second[z, block], q_slots[z], 0, block == 0)
 
-    def absorb_slot(d):
+    @pl.loop(4, max(n_sp, 4) + 1)
+    def _(hop):
+        for block in range(n_chip):
+            kv_hop(block, hop)
+
+    @pl.loop(1, n_sp)
+    def _(d):
         slot = sp_at(d)
         for block in range(n_chip):
-            for copy in kv_copies(block, slot, d):
-                copy.wait_recv()
             absorb(k_second[slot, block], v_second[slot, block], q_slots[z], 0, False)
 
-    times(1, n_sp, absorb_slot)
     loads[10].wait()
-    mixed = scatter_sum(2, dot(head_rows(run_out[0] / run_sum[0]), out_second[...]))
+    mixed = scatter_sum(2, head_rows(run_out[0] / run_sum[0]), out_second)
     decoded[...] = stream[...] + normed(mixed, post_second[...])
 
     for phase in range(3):
         gather_drain(phase)
+        sum_drain(phase)
     for c in range(CHUNKS):
         for _ in range(n_chip):
             src_copy(me, c, sib, 0).wait_send()
@@ -422,8 +500,7 @@
 
     def drain(d):
         for block in range(n_chip):
-            for copy in kv_copies(block, z, d):
-                copy.wait_send()
+            kv_drain(block, d)
         for copy in mix_copies(d, z):
             copy.wait_send()
 
@@ -452,6 +529,7 @@
     columns = query_first.shape[1] // HEAD * block_rows
     hidden_units = w_gate.shape[1]
     n_chip = n_tp // 2
+    span = width // PIECES
     dma = pltpu.SemaphoreType.DMA
     any_spec = pl.BlockSpec(memory_space=pl.ANY)
     vmem = pl.BlockSpec(memory_space=pltpu.VMEM)
@@ -466,8 +544,9 @@
             query_first, keyval_first, out_first, w_gate, w_value, w_down,
             query_second, keyval_second, out_second)),
         dma((11,)),
-        pltpu.VMEM((3, n_tp, rows, width), BF16),
-        dma((2, 3, n_tp)),
+        pltpu.VMEM((3, PIECES, n_tp, rows, span), BF16),
+        dma((3,)),
+        dma((3, PIECES, n_tp)),
         pltpu.VMEM((n_tp, CHUNKS, lines // CHUNKS, width), BF16),
         dma((2,)),
         dma((n_tp, CHUNKS)),
@@ -487,9 +566,13 @@
         pltpu.VMEM((n_sp, 2, columns), F32),
         pltpu.VMEM((n_sp, 2, columns), F32),
         dma((2, 2, n_sp)),
-        pltpu.VMEM((3, n_tp, rows, width), BF16),
-        pltpu.VMEM((3, n_tp, rows, width), BF16),
-        dma((2, 3, n_tp)),
+        pltpu.VMEM((3, PIECES, 2, n_chip, rows, span), BF16),
+        pltpu.VMEM((3, PIECES, n_chip, rows, span), BF16),
+        pltpu.VMEM((3, PIECES, n_chip, rows, span), BF16),
+        pltpu.VMEM((3, PIECES, n_chip, rows, span), BF16),
+        dma((3, 2)),
+        dma((3, PIECES)),
+        dma((3, PIECES, n_chip)),
         pltpu.VMEM((2, 16, hidden_units), BF16),
         pltpu.VMEM((2, 16, hidden_units), BF16),
         dma((2,)),

time: 121 us -> 105 us (0.87)
  the two profiles are of different devices: /device:TPU:23 before, /device:TPU:30 now
where the time goes in v2:
time: 105 us
  Pallas kernels  96 us (91%)
  local copies, waits for them, and re-layouts  9.25 us (9%)
    pallas_call x1, Pallas kernels, per_device(): pl.pallas_call(kernel, out_shape=jax.ShapeDtypeStruct((rows, width), F32)...  96 us
    unnamed x5, local copies, waits for them, and re-layouts  9.25 us

profile of v2, /device:TPU:30, one launch (start us, length us, event | category | flops | bytes accessed | tf_op | source)
XLA Modules:
  0.0 105.2 jit_solution(3147025750366289075)
XLA Ops:
  0.0 0.0 copy-start
  0.0 4.7 %copy.21.refs_9_ = bf16[2048,704]{1,0:T(8,128)(2,1)} copy(bf16[2048,704]{0,1:T(8,128)(2,1)} %param.29) | data formatting | bytes 5767168 | tf_op args[9]
  4.8 0.0 copy-done
  4.8 2.8 %copy.22.refs_10_ = bf16[2048,704]{1,0:T(8,128)(2,1)} copy(bf16[2048,704]{0,1:T(8,128)(2,1)S(1)} %copy-done) | data formatting | bytes 5767168 | tf_op args[10]
  7.6 96.0 %decoder.1 = f32[32,2048]{1,0:T(8,128)} custom-call(bf16[32,2048]{1,0:T(8,128)(2,1)} %refs_0_.1, bf16[256,2048]{1,0:T(8,128)(2,1)} %refs_1_.1, f32[1,2048]{1,0:T(1,128)} %bitcast.7, f32[1,2048]{1,0:T(1,128)} %bitcast.8, bf16[2048,512]{1,0:T(8,128)(2,1)} %refs_4_.1, bf16[2048,256]{1,0:T(8,128)(2,1)} %refs_5_.1, bf16[512,2048]{1,0:T(8,128)(2,1)} %refs_6_.1, ...), custom_call_target="tpu_custom_call" | custom-call | tf_op jit(solution)/shard_map/decoder/pallas_call | solution.py:585
  103.6 1.7 %copy.24 = f32[32,2048]{1,0:T(8,128)} copy(f32[32,2048]{1,0:T(8,128)} %decoder.1) | data formatting | bytes 524288
Async XLA Ops:
  0.0 4.8 %copy-start = (bf16[2048,704]{0,1:T(8,128)(2,1)S(1)}, bf16[2048,704]{0,1:T(8,128)(2,1)}, u32[]{:S(2)}) copy-start(bf16[2048,704]{0,1:T(8,128)(2,1)} %param.30) | copy-start | bytes 8650756
